TPU v7x, 32 devices: a whole 2x2x4 slice. The times are simulated.
32 devices in a mesh: ra: 4 (over z), cb: 4 (over y, x), dp: 2 (over core).
Axes of the slice: x: 2, y: 2, z: 4, core: 2. Of those that a mesh axis runs over, the one named last changes fastest.
Arguments:
- carried: bfloat16 [3072, 4096], P('dp', 'ra'), may hold values from -100 to 100
- branch_in: bfloat16 [3072, 4096], P('dp', 'ra'), may hold values from -12 to 12
- gain_in: float32 [4096], P('ra'), may hold values from 0.1 to 1.9
- bias_in: float32 [4096], P('ra'), may hold values from -1.8 to 1.8
- up_weight: bfloat16 [4096, 16384], P('ra', 'cb'), may hold values from -0.125 to 0.125
- down_weight: bfloat16 [16384, 4096], P('cb', 'ra'), may hold values from -0.046875 to 0.046875
- gain_out: float32 [4096], P('ra'), may hold values from 0.1 to 1.9
- bias_out: float32 [4096], P('ra'), may hold values from -1.8 to 1.8
Outputs:
- layer_out: bfloat16 [3072, 4096], P('dp', 'ra')
All inputs are finite; a program needn't handle non-finite values.
Results may differ from a plain program's by a relative error of at most 0.006.
Values may be sent and summed in bfloat16 or wider, within the bound.
A program may use at most 128 MiB of HBM per device.

v0:
```python
import jax
import jax.numpy as jnp
from jax import lax
from jax.sharding import PartitionSpec as P

residual_scale = 2.0**0.25
norm_eps = 1e-05


def normalize(mixed, totals, squares, width, gain, bias):
    mean = totals[:, None] / width
    spread = squares[:, None] / width - mean * mean
    return (mixed - mean) * lax.rsqrt(spread + norm_eps) * gain + bias


def per_device(carried, branch_in, gain_in, bias_in, up_weight, down_weight, gain_out, bias_out):
    width = carried.shape[1] * lax.axis_size("ra")
    mixed_in = residual_scale * carried.astype(jnp.float32) + branch_in.astype(jnp.float32)
    totals, squares = lax.psum(
        (jnp.sum(mixed_in, axis=1), jnp.sum(mixed_in * mixed_in, axis=1)), "ra"
    )
    normed = normalize(mixed_in, totals, squares, width, gain_in, bias_in).astype(jnp.bfloat16)
    regrouped = lax.all_to_all(up_weight, "ra", split_axis=1, concat_axis=0, tiled=True)
    pre_share = lax.dot_general(
        regrouped,
        lax.all_gather(normed, "ra", axis=1, tiled=True),
        (((0,), (1,)), ((), ())),
        preferred_element_type=jnp.float32,
    )
    hidden_share = jnp.square(jnp.maximum(pre_share, 0.0)).astype(jnp.bfloat16)
    branch_part = lax.dot_general(
        lax.all_gather(hidden_share, "ra", axis=0, tiled=True),
        down_weight,
        (((0,), (0,)), ((), ())),
        preferred_element_type=jnp.float32,
    )
    branch_out = lax.psum(branch_part, "cb")
    mixed_out = residual_scale * normed.astype(jnp.float32) + branch_out
    totals_out, squares_out = lax.psum(
        (jnp.sum(mixed_out, axis=1), jnp.sum(mixed_out * mixed_out, axis=1)), "ra"
    )
    return normalize(mixed_out, totals_out, squares_out, width, gain_out, bias_out).astype(
        jnp.bfloat16
    )


def solution(mesh):
    in_specs = (
        P("dp", "ra"),
        P("dp", "ra"),
        P("ra"),
        P("ra"),
        P("ra", "cb"),
        P("cb", "ra"),
        P("ra"),
        P("ra"),
    )
    out_specs = P("dp", "ra")
    return jax.shard_map(
        per_device, mesh=mesh, in_specs=in_specs, out_specs=out_specs, check_vma=False
    )
```

profile of v0, /device:TPU:0, one launch (start us, length us, event | category | flops | bytes accessed | tf_op | source)
XLA Modules:
  0.0 859.6 jit_solution(17207012379904280185)
XLA Ops:
  6.5 0.0 copy-start.1
  6.5 0.0 copy-start.2
  6.5 0.0 copy-start.3
  6.5 0.0 all-gather.3.cloned.1.call-start
  6.5 4.5 fusion
  11.1 20.5 %all-reduce.1 = (f32[1536]{0:T(1024)S(1)}, f32[1536]{0:T(1024)S(1)}) all-reduce(f32[1536]{0:T(1024)S(1)} %get-tuple-element.8, f32[1536]{0:T(1024)S(1)} %get-tuple-element.7), channel_id=1, replica_groups=mesh['ra'=4,'cb'=4,'dp'=2] {'ra'}, use_global_device_ids=true, to_apply=%region_3.0 | all-reduce | flops 3072 | bytes 24576 | tf_op jit(solution)/shard_map/psum | solution.py:19
  31.6 0.0 copy-done.1
  31.6 0.0 copy-done.2
  31.6 0.0 copy-done.3
  31.6 4.5 add_convert_fusion.1
  36.2 0.0 all-gather.3.cloned.1.call-update
  36.2 0.0 all-gather.5.cloned.1.call-start
  36.2 12.2 %copy.9 = bf16[1024,4096]{0,1:T(8,128)(2,1)} copy(bf16[1024,4096]{1,0:T(8,128)(2,1)} %param.12) | data formatting | bytes 16777216 | tf_op args[4]
  48.5 373.1 %all_to_all.19 = bf16[1024,4,1024]{0,2,1:T(8,128)(2,1)} all-to-all(bf16[1024,4,1024]{0,2,1:T(8,128)(2,1)} %bitcast.10), channel_id=1, replica_groups=mesh['ra'=4,'cb'=4,'dp'=2] {'ra'}, dimensions={1} | all-to-all | bytes 16777216 | tf_op jit(solution)/shard_map/all_to_all | solution.py:23
  421.6 11.4 %copy.10 = bf16[4,1024,1024]{2,1,0:T(8,128)(2,1)} copy(bf16[4,1024,1024]{1,2,0:T(8,128)(2,1)} %bitcast.9) | data formatting | bytes 16777216 | tf_op jit(solution)/shard_map/all_to_all | solution.py:23
  432.9 0.0 all-gather.3.cloned.1.call-done
  432.9 19.2 %fusion.1 = bf16[1024,1536]{0,1:T(8,128)(2,1)} fusion(bf16[1536,4096]{1,0:T(8,128)(2,1)} %all-gather.3.cloned.1.call-done, bf16[4096,1024]{1,0:T(8,128)(2,1)} %bitcast.11), kind=kOutput, calls=%fused_computation.8 | convolution fusion | flops 12889620480 | bytes 24117248 | tf_op jit(solution)/shard_map/dot_general | solution.py:24
  452.1 0.0 all-gather.5.cloned.1.call-update
  452.1 0.2 all-reduce.4.cloned.1.call-start
  452.3 216.9 %all-gather.5.cloned.1.call-done = bf16[4096,1536]{0,1:T(8,128)(2,1)} async-done(((bf16[1024,1536]{0,1:T(8,128)(2,1)}), bf16[4096,1536]{0,1:T(8,128)(2,1)}) %all-gather.5.cloned.1.call-update) | async-done | bytes 12582928 | tf_op jit(solution)/shard_map/all_gather | solution.py:32
  669.2 19.5 %fusion.3 = f32[1536,1024]{1,0:T(8,128)} fusion(bf16[4096,1536]{0,1:T(8,128)(2,1)} %all-gather.5.cloned.1.call-done, bf16[4096,1024]{1,0:T(8,128)(2,1)} %param.13), kind=kOutput, calls=%fused_computation.14 | convolution fusion | flops 12884901888 | bytes 27262976 | tf_op jit(solution)/shard_map/dot_general | solution.py:31
  688.7 0.0 copy-start
  688.7 0.0 all-reduce.4.cloned.1.call-update
  688.8 0.0 copy-start.4
  688.8 0.0 copy-start.5
  688.8 136.5 %all-reduce.4.cloned.1.call-done = f32[1536,1024]{1,0:T(8,128)} async-done(((f32[1536,1024]{1,0:T(8,128)}), f32[1536,1024]{1,0:T(8,128)}) %all-reduce.4.cloned.1.call-update) | async-done | bytes 6291472 | tf_op jit(solution)/shard_map/psum | solution.py:37
  825.3 0.0 copy-done
  825.3 4.1 fusion.2
  829.4 18.7 %all-reduce = (f32[1536]{0:T(1024)S(1)}, f32[1536]{0:T(1024)S(1)}) all-reduce(f32[1536]{0:T(1024)S(1)} %get-tuple-element.6, f32[1536]{0:T(1024)S(1)} %get-tuple-element.5), channel_id=1, replica_groups=mesh['ra'=4,'cb'=4,'dp'=2] {'ra'}, use_global_device_ids=true, to_apply=%region_8.0 | all-reduce | flops 3072 | bytes 24576 | tf_op jit(solution)/shard_map/psum | solution.py:39
  848.1 0.0 copy-done.4
  848.1 0.0 copy-done.5
  848.1 4.9 add_convert_fusion
  (2 shorter events, 0.0 us)
Async XLA Ops:
  6.5 25.1 %copy-start.1 = (bf16[1536,1024]{1,0:T(8,128)(2,1)S(1)}, bf16[1536,1024]{1,0:T(8,128)(2,1)}, u32[]{:S(2)}) copy-start(bf16[1536,1024]{1,0:T(8,128)(2,1)} %param.9) | copy-start | bytes 9437188
  6.5 25.1 %copy-start.2 = (f32[1024]{0:T(1024)S(1)}, f32[1024]{0:T(1024)}, u32[]{:S(2)}) copy-start(f32[1024]{0:T(1024)} %param.11) | copy-start | bytes 12292
  6.5 25.1 %copy-start.3 = (f32[1024]{0:T(1024)S(1)}, f32[1024]{0:T(1024)}, u32[]{:S(2)}) copy-start(f32[1024]{0:T(1024)} %param.10) | copy-start | bytes 12292
  6.5 426.4 %all-gather.3.cloned.1.call-start = ((), (), s32[]{:S(2)}) async-start(), calls=%async_computation.1 | async-start | bytes 15728640 | tf_op jit(solution)/shard_map/all_gather | solution.py:26
  36.2 633.1 %all-gather.5.cloned.1.call-start = ((), (), s32[]{:S(2)}) async-start(), calls=%async_computation.2 | async-start | bytes 15728640 | tf_op jit(solution)/shard_map/all_gather | solution.py:32
  452.1 373.1 %all-reduce.4.cloned.1.call-start = ((), (), s32[]{:S(2)}) async-start(), calls=%async_computation.3 | async-start | bytes 12582912 | tf_op jit(solution)/shard_map/psum | solution.py:37
  688.7 136.5 %copy-start = (bf16[1536,1024]{1,0:T(8,128)(2,1)S(1)}, bf16[1536,1024]{1,0:T(8,128)(2,1)}, u32[]{:S(2)}) copy-start(bf16[1536,1024]{1,0:T(8,128)(2,1)} %add_convert_fusion.1) | copy-start | bytes 9437188
  688.8 159.4 %copy-start.4 = (f32[1024]{0:T(1024)S(1)}, f32[1024]{0:T(1024)}, u32[]{:S(2)}) copy-start(f32[1024]{0:T(1024)} %param.15) | copy-start | bytes 12292
  688.8 159.4 %copy-start.5 = (f32[1024]{0:T(1024)S(1)}, f32[1024]{0:T(1024)}, u32[]{:S(2)}) copy-start(f32[1024]{0:T(1024)} %param.14) | copy-start | bytes 12292
Sparse Core Ops, SparseCore 0:
  36.3 395.6 all-gather.2
  452.2 216.9 all-gather.4
  688.9 136.3 all-reduce.3
where the time goes:
time: 860 us
  blocking collectives  412 us (48%)
  waiting for transfers between devices  353 us (41%)
  matrix products  38.6 us (4%)
  local copies, waits for them, and re-layouts  23.6 us (3%)
  other arithmetic  18.1 us (2%)
  between operations  13.2 us (2%)
    all_to_all x1, blocking collectives, per_device(): lax.all_to_all(up_weight, 'ra', split_axis=1, concat_axis=0, tiled=True)  373 us
    all_gather x1, waiting for transfers between devices, per_device(): lax.all_gather(hidden_share, 'ra', axis=0, tiled=True)  217 us
    psum x1, waiting for transfers between devices, per_device(): branch_out = lax.psum(branch_part, 'cb')  136 us
    psum x1, blocking collectives, per_device(): lax.psum((jnp.sum(mixed_in, axis=1), jnp.sum(mixed_in * mixed_in, axis=1)...  20.5 us
    dot_general x1, matrix products, per_device(): lax.dot_general(lax.all_gather(hidden_share, 'ra', axis=0, tiled=True), d...  19.5 us
    dot_general x1, matrix products, per_device(): lax.dot_general(regrouped, lax.all_gather(normed, 'ra', axis=1, tiled=Tru...  19.2 us
    psum x1, blocking collectives, per_device(): lax.psum((jnp.sum(mixed_out, axis=1), jnp.sum(mixed_out * mixed_out, axis...  18.7 us
  transfers between devices with their start and end apart: 3, of which 2 were waited for; matrix products, arithmetic and copies ran while one was open for 3% of the time, Pallas kernels for 0%

commit v1 on v0

--- a/solution.py
+++ b/solution.py
@@ -5,6 +5,14 @@
 
 residual_scale = 2.0**0.25
 norm_eps = 1e-05
+
+
+def doubling_sum(shard, mesh_axis):
+    devices, acc = (lax.axis_size(mesh_axis), shard)
+    for reach in [1 << k for k in range(devices.bit_length() - 1)]:
+        pairs = [(i, i ^ reach) for i in range(devices)]
+        acc = acc + lax.ppermute(acc, mesh_axis, pairs)
+    return acc
 
 
 def normalize(mixed, totals, squares, width, gain, bias):
@@ -34,7 +42,7 @@
         (((0,), (0,)), ((), ())),
         preferred_element_type=jnp.float32,
     )
-    branch_out = lax.psum(branch_part, "cb")
+    branch_out = doubling_sum(branch_part, "cb")
     mixed_out = residual_scale * normed.astype(jnp.float32) + branch_out
     totals_out, squares_out = lax.psum(
         (jnp.sum(mixed_out, axis=1), jnp.sum(mixed_out * mixed_out, axis=1)), "ra"

time: 860 us -> 1010 us (1.17)
  waiting for transfers between devices: 353 us -> 488 us
  local copies, waits for them, and re-layouts: 23.6 us -> 34.3 us
    ppermute x0 -> x2, waiting for transfers between devices: none -> 271 us  [doubling_sum(): acc = acc + lax.ppermute(acc, mesh_axis, pairs)]
    psum x1 -> x0, waiting for transfers between devices: 136 us -> none  [per_device(): branch_out = lax.psum(branch_part, 'cb')]
  transfers between devices with their start and end apart: 3 -> 4, of which waited for: 2 -> 3; matrix products, arithmetic and copies ran while one was open for 3% -> 2% of each run, Pallas kernels for 0% -> 0%
where the time goes in v1:
time: 1010 us; the launch traced here: 1000 us
  waiting for transfers between devices  488 us (48%)
  blocking collectives  409 us (40%)
  matrix products  37.1 us (4%)
  local copies, waits for them, and re-layouts  34.3 us (3%)
  other arithmetic  19.3 us (2%)
  between operations  13.5 us (1%)
    all_to_all x1, blocking collectives, per_device(): lax.all_to_all(up_weight, 'ra', split_axis=1, concat_axis=0, tiled=True)  373 us
    ppermute x2, waiting for transfers between devices, doubling_sum(): acc = acc + lax.ppermute(acc, mesh_axis, pairs)  271 us
    all_gather x1, waiting for transfers between devices, per_device(): lax.all_gather(hidden_share, 'ra', axis=0, tiled=True)  217 us
    psum x1, blocking collectives, per_device(): lax.psum((jnp.sum(mixed_in, axis=1), jnp.sum(mixed_in * mixed_in, axis=1)...  20.5 us
  transfers between devices with their start and end apart: 4, of which 3 were waited for; matrix products, arithmetic and copies ran while one was open for 2% of the time, Pallas kernels for 0%

profile of v1, /device:TPU:0, one launch (start us, length us, event | category | flops | bytes accessed | tf_op | source)
XLA Modules:
  0.0 1005.0 jit_solution(14767584129587551216)
XLA Ops:
  6.5 0.0 all-gather.3.cloned.1.call-start
  6.5 3.2 copy.15
  9.7 0.0 copy-start.1
  9.7 0.0 copy-start.2
  9.7 4.6 copy.16
  14.4 3.3 fusion
  17.7 20.5 %all-reduce.1 = (f32[1536]{0:T(1024)S(1)}, f32[1536]{0:T(1024)S(1)}) all-reduce(f32[1536]{0:T(1024)S(1)} %get-tuple-element.8, f32[1536]{0:T(1024)S(1)} %get-tuple-element.7), channel_id=1, replica_groups=mesh['ra'=4,'cb'=4,'dp'=2] {'ra'}, use_global_device_ids=true, to_apply=%region_3.0 | all-reduce | flops 3072 | bytes 24576 | tf_op jit(solution)/shard_map/psum | solution.py:27
  38.3 0.0 copy-done.1
  38.3 0.0 copy-done.2
  38.3 4.6 add_convert_fusion.1
  42.9 0.0 all-gather.3.cloned.1.call-update
  42.9 0.0 all-gather.5.cloned.1.call-start
  42.9 12.3 %copy.17 = bf16[1024,4096]{0,1:T(8,128)(2,1)} copy(bf16[1024,4096]{1,0:T(8,128)(2,1)} %param.12) | data formatting | bytes 16777216 | tf_op args[4]
  55.2 373.1 %all_to_all.19 = bf16[1024,4,1024]{0,2,1:T(8,128)(2,1)} all-to-all(bf16[1024,4,1024]{0,2,1:T(8,128)(2,1)} %bitcast.10), channel_id=1, replica_groups=mesh['ra'=4,'cb'=4,'dp'=2] {'ra'}, dimensions={1} | all-to-all | bytes 16777216 | tf_op jit(solution)/shard_map/all_to_all | solution.py:31
  428.3 11.4 %copy.18 = bf16[4,1024,1024]{2,1,0:T(8,128)(2,1)} copy(bf16[4,1024,1024]{1,2,0:T(8,128)(2,1)} %bitcast.9) | data formatting | bytes 16777216 | tf_op jit(solution)/shard_map/all_to_all | solution.py:31
  439.6 0.0 all-gather.3.cloned.1.call-done
  439.6 19.2 %fusion.1 = bf16[1024,1536]{0,1:T(8,128)(2,1)} fusion(bf16[1536,4096]{0,1:T(8,128)(2,1)} %all-gather.3.cloned.1.call-done, bf16[4096,1024]{1,0:T(8,128)(2,1)} %bitcast.11), kind=kOutput, calls=%fused_computation.8 | convolution fusion | flops 12889620480 | bytes 24117248 | tf_op jit(solution)/shard_map/dot_general | solution.py:32
  458.9 0.0 all-gather.5.cloned.1.call-update
  458.9 217.1 %all-gather.5.cloned.1.call-done = bf16[4096,1536]{0,1:T(8,128)(2,1)} async-done(((bf16[1024,1536]{0,1:T(8,128)(2,1)}), bf16[4096,1536]{0,1:T(8,128)(2,1)}) %all-gather.5.cloned.1.call-update) | async-done | bytes 12582928 | tf_op jit(solution)/shard_map/all_gather | solution.py:40
  676.0 17.9 %fusion.3 = f32[1536,1024]{0,1:T(8,128)S(1)} fusion(bf16[4096,1536]{0,1:T(8,128)(2,1)} %all-gather.5.cloned.1.call-done, bf16[4096,1024]{1,0:T(8,128)(2,1)} %param.13), kind=kOutput, calls=%fused_computation.14 | convolution fusion | flops 12884901888 | bytes 27262976 | tf_op jit(solution)/shard_map/dot_general | solution.py:39
  694.0 0.0 copy-start
  694.0 1.5 collective-permute-start
  695.5 136.1 %collective-permute-done = f32[1536,1024]{0,1:T(8,128)} collective-permute-done((f32[1536,1024]{0,1:T(8,128)S(1)}, f32[1536,1024]{0,1:T(8,128)}, u32[]{:S(2)}, u32[]{:S(2)}) %collective-permute-start) | collective-permute-done | bytes 6291488 | tf_op jit(solution)/shard_map/ppermute | solution.py:14
  831.6 4.2 add.48
  835.8 0.0 copy-start.3
  835.8 0.0 copy-start.4
  835.8 1.5 collective-permute-start.1
  837.3 135.1 %collective-permute-done.1 = f32[1536,1024]{0,1:T(8,128)S(1)} collective-permute-done((f32[1536,1024]{0,1:T(8,128)S(1)}, f32[1536,1024]{0,1:T(8,128)S(1)}, u32[]{:S(2)}, u32[]{:S(2)}) %collective-permute-start.1) | collective-permute-done | bytes 6291488 | tf_op jit(solution)/shard_map/ppermute | solution.py:14
  972.4 0.0 copy-done
  972.4 3.7 fusion.2
  976.1 15.7 %all-reduce = (f32[1536]{0:T(1024)S(1)}, f32[1536]{0:T(1024)S(1)}) all-reduce(f32[1536]{0:T(1024)S(1)} %get-tuple-element.6, f32[1536]{0:T(1024)S(1)} %get-tuple-element.5), channel_id=1, replica_groups=mesh['ra'=4,'cb'=4,'dp'=2] {'ra'}, use_global_device_ids=true, to_apply=%region_7.0 | all-reduce | flops 3072 | bytes 24576 | tf_op jit(solution)/shard_map/psum | solution.py:47
  991.8 0.0 copy-done.3
  991.8 0.0 copy-done.4
  991.8 3.5 add_convert_fusion
  995.3 2.9 copy.19
  (2 shorter events, 0.0 us)
Async XLA Ops:
  6.5 433.1 %all-gather.3.cloned.1.call-start = ((), (), s32[]{:S(2)}) async-start(), calls=%async_computation.1 | async-start | bytes 15728640 | tf_op jit(solution)/shard_map/all_gather | solution.py:34
  9.7 28.5 %copy-start.1 = (f32[1024]{0:T(1024)S(1)}, f32[1024]{0:T(1024)}, u32[]{:S(2)}) copy-start(f32[1024]{0:T(1024)} %param.11) | copy-start | bytes 12292
  9.7 28.5 %copy-start.2 = (f32[1024]{0:T(1024)S(1)}, f32[1024]{0:T(1024)}, u32[]{:S(2)}) copy-start(f32[1024]{0:T(1024)} %param.10) | copy-start | bytes 12292
  42.9 633.1 %all-gather.5.cloned.1.call-start = ((), (), s32[]{:S(2)}) async-start(), calls=%async_computation.2 | async-start | bytes 15728640 | tf_op jit(solution)/shard_map/all_gather | solution.py:40
  694.0 278.4 %copy-start = (bf16[1536,1024]{0,1:T(8,128)(2,1)S(1)}, bf16[1536,1024]{0,1:T(8,128)(2,1)}, u32[]{:S(2)}) copy-start(bf16[1536,1024]{0,1:T(8,128)(2,1)} %add_convert_fusion.1) | copy-start | bytes 9437188
  694.0 137.6 %collective-permute-start = (f32[1536,1024]{0,1:T(8,128)S(1)}, f32[1536,1024]{0,1:T(8,128)}, u32[]{:S(2)}, u32[]{:S(2)}) collective-permute-start(f32[1536,1024]{0,1:T(8,128)S(1)} %fusion.3), channel_id=1, source_target_pairs={{0,2},{2,0},{4,6},{6,4},{1,3},{3,1},{5,7},{7,5},{8,10},{10,8},{12,... | collective-permute-start | bytes 18874376 | tf_op jit(solution)/shard_map/ppermute | solution.py:14
  835.8 156.0 %copy-start.3 = (f32[1024]{0:T(1024)S(1)}, f32[1024]{0:T(1024)}, u32[]{:S(2)}) copy-start(f32[1024]{0:T(1024)} %param.15) | copy-start | bytes 12292
  835.8 156.0 %copy-start.4 = (f32[1024]{0:T(1024)S(1)}, f32[1024]{0:T(1024)}, u32[]{:S(2)}) copy-start(f32[1024]{0:T(1024)} %param.14) | copy-start | bytes 12292
  835.8 136.6 %collective-permute-start.1 = (f32[1536,1024]{0,1:T(8,128)S(1)}, f32[1536,1024]{0,1:T(8,128)S(1)}, u32[]{:S(2)}, u32[]{:S(2)}) collective-permute-start(f32[1536,1024]{0,1:T(8,128)S(1)} %add.48), channel_id=1, source_target_pairs={{0,4},{2,6},{4,0},{6,2},{1,5},{3,7},{5,1},{7,3},{8,12},{10,14},{12... | collective-permute-start | bytes 18874376 | tf_op jit(solution)/shard_map/ppermute | solution.py:14
Sparse Core Ops, SparseCore 0:
  43.0 395.6 all-gather.2
  459.0 216.9 all-gather.4
